TPU v7x, 32 devices: a whole 2x2x4 slice. The times are simulated.
32 devices in a mesh: dp: 4 (over y, x), kv: 4 (over z), tp: 2 (over core).
Axes of the slice: x: 2, y: 2, z: 4, core: 2. Of those that a mesh axis runs over, the one named last changes fastest.
Arguments:
- tokens: bfloat16 [32, 2048], P('dp', 'kv'), may hold values from -6 to 6
- pre_gain: float32 [2048], P('kv'), may hold values from 0.1 to 1.9
- query_weight: bfloat16 [2048, 1024], P('kv', 'tp'), may hold values from -0.125 to 0.125
- key_weight: bfloat16 [2048, 1024], P('kv', 'tp'), may hold values from -0.125 to 0.125
- value_weight: bfloat16 [2048, 1024], P('kv', 'tp'), may hold values from -0.125 to 0.125
- outgate_weight: bfloat16 [2048, 1024], P('kv', 'tp'), may hold values from -0.125 to 0.125
- input_gate_weight: bfloat16 [2048, 4], replicated, may hold values from -0.125 to 0.125
- forget_gate_weight: bfloat16 [2048, 4], replicated, may hold values from -0.125 to 0.125
- cache_keys: bfloat16 [32, 64, 1024], P(('dp', 'kv'), None, 'tp'), may hold values from -6 to 6
- cache_values: bfloat16 [32, 64, 1024], P(('dp', 'kv'), None, 'tp'), may hold values from -6 to 6
- cache_input: float32 [32, 64, 4], P(('dp', 'kv'), None, 'tp'), may hold values from -6 to 250
- cache_forget: float32 [32, 64, 4], P(('dp', 'kv'), None, 'tp'), may hold values from -0.7 to 0
- lengths: int32 [32], P(('dp', 'kv')), may hold values from 1 to 64, 819 in all
- state_matrix: float32 [32, 4, 256, 256], P(('dp', 'kv'), 'tp'), may hold values from -6 to 6
- state_norm: float32 [32, 4, 256], P(('dp', 'kv'), 'tp'), may hold values from -6 to 6
- state_max: float32 [32, 4], P(('dp', 'kv'), 'tp'), may hold values from -4 to 253
- head_gain: float32 [1024], P('tp'), may hold values from 0.1 to 1.9
- out_weight: bfloat16 [1024, 2048], P('tp', 'kv'), may hold values from -0.375 to 0.375
- mixer_gain: float32 [2048], replicated, may hold values from 0.1 to 1.9
- gate_weight: bfloat16 [2048, 5632], P(None, ('kv', 'tp')), may hold values from -0.125 to 0.125
- up_weight: bfloat16 [2048, 5632], P(None, ('kv', 'tp')), may hold values from -0.125 to 0.125
- down_weight: bfloat16 [5632, 2048], P(('kv', 'tp')), may hold values from -0.21875 to 0.21875
Outputs:
- layer_out: bfloat16 [32, 2048], P('dp', ('kv', 'tp'))
Inputs may be any that keep to these rules, and one draw needn't show every extreme that they name: `lengths`: positions from a sequence's length on take no part.
All inputs are finite; a program needn't handle non-finite values. No bound on the sum of `lengths` on one device may be relied on, other than what follows from the above.
Results may differ from a plain program's by a relative error of at most 0.018.
Values may be sent and summed in bfloat16 or wider, within the bound.
A program may use at most 64 MiB of HBM per device.

v0:
```python
import jax
import jax.numpy as jnp
from jax import lax
from jax.sharding import PartitionSpec as P

EPS = 1e-06


def per_device(
    tokens,
    pre_gain,
    query_weight,
    key_weight,
    value_weight,
    outgate_weight,
    input_gate_weight,
    forget_gate_weight,
    cache_keys,
    cache_values,
    cache_input,
    cache_forget,
    lengths,
    state_matrix,
    state_norm,
    state_max,
    head_gain,
    out_weight,
    mixer_gain,
    gate_weight,
    up_weight,
    down_weight,
):
    col_width = tokens.shape[1]
    own_seqs = cache_keys.shape[0]
    block_len = cache_keys.shape[1]
    head_count = state_max.shape[1]
    head_size = state_norm.shape[2]
    shard_index = lax.axis_index("kv")
    half_index = lax.axis_index("tp")
    kv_count = lax.axis_size("kv")
    model_width = col_width * kv_count
    token_values = tokens.astype(jnp.float32)
    squares = jnp.sum(token_values * token_values, axis=1)
    normed = (token_values * pre_gain[None, :]).astype(jnp.bfloat16)
    corner = (shard_index * col_width, half_index * head_count)
    gate_pair = jnp.concatenate(
        [
            lax.dynamic_slice(input_gate_weight, corner, (col_width, head_count)),
            lax.dynamic_slice(forget_gate_weight, corner, (col_width, head_count)),
        ],
        axis=1,
    )

    def product(weight):
        return jnp.dot(normed, weight, preferred_element_type=jnp.float32)

    query_term = product(query_weight)
    key_term = product(key_weight)
    value_term = product(value_weight)
    outgate_term = product(outgate_weight)
    gate_term = product(gate_pair)
    square_totals = lax.psum(squares, "kv")
    query_sum, key_sum, value_sum, outgate_sum, gate_sum = (
        lax.psum_scatter(query_term, "kv", scatter_dimension=0, tiled=True),
        lax.psum_scatter(key_term, "kv", scatter_dimension=0, tiled=True),
        lax.psum_scatter(value_term, "kv", scatter_dimension=0, tiled=True),
        lax.psum_scatter(outgate_term, "kv", scatter_dimension=0, tiled=True),
        lax.psum_scatter(gate_term, "kv", scatter_dimension=0, tiled=True),
    )
    own_squares = lax.dynamic_slice_in_dim(square_totals, shard_index * own_seqs, own_seqs, 0)
    scale_first = lax.rsqrt(own_squares / model_width + EPS)[:, None]
    query = (scale_first * query_sum).astype(jnp.bfloat16)
    keys_new = (scale_first * key_sum).astype(jnp.bfloat16)
    values_new = (scale_first * value_sum).astype(jnp.bfloat16)
    outgate = (scale_first * outgate_sum).astype(jnp.bfloat16)
    gate_values = scale_first * gate_sum
    in_gate = gate_values[:, :head_count]
    forget_new = jax.nn.log_sigmoid(gate_values[:, head_count:])
    query_heads = query.reshape(own_seqs, head_count, head_size)
    key_heads = keys_new.reshape(own_seqs, head_count, head_size)
    value_heads = values_new.reshape(own_seqs, head_count, head_size)
    cached_keys = cache_keys.reshape(own_seqs, block_len, head_count, head_size)
    cached_values = cache_values.reshape(own_seqs, block_len, head_count, head_size)
    inv_root = head_size ** (-0.5)
    live_mask = (lax.broadcasted_iota(jnp.int32, (own_seqs, block_len), 1) < lengths[:, None])[
        :, :, None
    ]
    forget_live = jnp.where(live_mask, cache_forget, jnp.float32(0.0))
    running = jnp.cumsum(forget_live, axis=1)
    total_log = running[:, -1, :] + forget_new
    weight_log = jnp.where(live_mask, total_log[:, None, :] - running + cache_input, -jnp.inf)
    state_log = total_log + state_max
    peak_log = jnp.maximum(jnp.maximum(state_log, in_gate), jnp.max(weight_log, axis=1))
    key_dots = (
        jnp.einsum("shd,slhd->slh", query_heads, cached_keys, preferred_element_type=jnp.float32)
        * inv_root
    )
    block_scores = jnp.exp(weight_log - peak_log[:, None, :]) * key_dots
    query_scaled = query_heads.astype(jnp.float32) * inv_root
    self_score = jnp.exp(in_gate - peak_log) * jnp.sum(
        query_scaled * key_heads.astype(jnp.float32), axis=2
    )
    carried = jnp.exp(state_log - peak_log)
    block_weights = block_scores.astype(jnp.bfloat16)
    memory_read = jnp.einsum(
        "shvd,shd->shv", state_matrix, query_scaled, precision=lax.Precision.HIGHEST
    )
    norm_read = jnp.einsum("shd,shd->sh", state_norm, query_scaled, precision=lax.Precision.HIGHEST)
    numerator = (
        carried[:, :, None] * memory_read
        + jnp.einsum(
            "slh,slhd->shd", block_weights, cached_values, preferred_element_type=jnp.float32
        )
        + self_score[:, :, None] * value_heads.astype(jnp.float32)
    )
    denominator = carried * norm_read + jnp.sum(block_scores, axis=1) + self_score
    hidden = numerator / jnp.maximum(jnp.abs(denominator), 1.0)[:, :, None]
    mixed_heads = (
        hidden.reshape(own_seqs, head_count * head_size)
        * head_gain[None, :]
        * jax.nn.sigmoid(outgate.astype(jnp.float32))
    ).astype(jnp.bfloat16)
    mix_terms = jnp.dot(
        lax.all_gather(mixed_heads, "kv", axis=0, tiled=True),
        out_weight,
        preferred_element_type=jnp.float32,
    )
    mix_sum = lax.psum_scatter(
        mix_terms.astype(jnp.bfloat16), "tp", scatter_dimension=1, tiled=True
    ).astype(jnp.float32)
    narrow = mix_sum.shape[1]
    residual = (
        lax.dynamic_slice_in_dim(token_values, half_index * narrow, narrow, 1) + mix_sum
    ).astype(jnp.bfloat16)
    piece_wide = lax.all_gather(residual, ("kv", "tp"), axis=1, tiled=True).astype(jnp.float32)
    normed_piece = (piece_wide * mixer_gain[None, :]).astype(jnp.bfloat16)
    gate_acc = jnp.dot(normed_piece, gate_weight, preferred_element_type=jnp.float32)
    up_acc = jnp.dot(normed_piece, up_weight, preferred_element_type=jnp.float32)
    sum_squares = jnp.sum(piece_wide * piece_wide, axis=1)
    gate_acc, up_acc, sum_squares = (gate_acc, up_acc, sum_squares)
    scale_mid = lax.rsqrt(sum_squares / model_width + EPS)[:, None]
    hidden_units = (jax.nn.silu(scale_mid * gate_acc) * (scale_mid * up_acc)).astype(jnp.bfloat16)
    summed = lax.psum_scatter(
        lax.dot_general(
            down_weight, hidden_units, (((0,), (1,)), ((), ())), preferred_element_type=jnp.float32
        ),
        ("kv", "tp"),
        scatter_dimension=0,
        tiled=True,
    )
    mixer_out = summed.T
    return (residual.astype(jnp.float32) + mixer_out).astype(jnp.bfloat16)


def solution(mesh):
    in_specs = (
        P("dp", "kv"),
        P("kv"),
        P("kv", "tp"),
        P("kv", "tp"),
        P("kv", "tp"),
        P("kv", "tp"),
        P(),
        P(),
        P(("dp", "kv"), None, "tp"),
        P(("dp", "kv"), None, "tp"),
        P(("dp", "kv"), None, "tp"),
        P(("dp", "kv"), None, "tp"),
        P(("dp", "kv")),
        P(("dp", "kv"), "tp", None, None),
        P(("dp", "kv"), "tp", None),
        P(("dp", "kv"), "tp"),
        P("tp"),
        P("tp", "kv"),
        P(),
        P(None, ("kv", "tp")),
        P(None, ("kv", "tp")),
        P(("kv", "tp"), None),
    )
    out_specs = P("dp", ("kv", "tp"))
    return jax.shard_map(
        per_device, mesh=mesh, in_specs=in_specs, out_specs=out_specs, check_vma=False
    )
```

profile of v0, /device:TPU:0, one launch (start us, length us, event | category | flops | bytes accessed | tf_op | source)
XLA Modules:
  0.0 147.6 jit_solution(3637259032463186697)
XLA Ops:
  6.6 1.6 %multiply_reduce_fusion = f32[8]{0:T(128)} fusion(bf16[8,512]{1,0:T(8,128)(2,1)} %param.22), kind=kLoop, calls=%fused_computation.22 | loop fusion | flops 12280 | bytes 8224 | tf_op jit(solution)/shard_map/reduce_sum | solution.py:43
  8.2 1.9 %fusion.43 = f32[8,512]{1,0:T(8,128)} fusion(bf16[512,512]{1,0:T(8,128)(2,1)} %param.27, f32[512]{0:T(512)} %param.23, bf16[8,512]{1,0:T(8,128)(2,1)} %param.22), kind=kOutput, calls=%fused_computation.73 | convolution fusion | flops 4206592 | bytes 550912 | tf_op jit(solution)/shard_map/dot_general | solution.py:55
  10.0 1.9 %fusion.44 = f32[8,512]{1,0:T(8,128)} fusion(bf16[512,512]{1,0:T(8,128)(2,1)} %param.26, f32[512]{0:T(512)} %param.23, bf16[8,512]{1,0:T(8,128)(2,1)} %param.22), kind=kOutput, calls=%fused_computation.74 | convolution fusion | flops 4206592 | bytes 550912 | tf_op jit(solution)/shard_map/dot_general | solution.py:55
  11.9 1.9 %fusion.46 = f32[8,512]{1,0:T(8,128)} fusion(bf16[512,512]{1,0:T(8,128)(2,1)} %param.24, f32[512]{0:T(512)} %param.23, bf16[8,512]{1,0:T(8,128)(2,1)} %param.22), kind=kOutput, calls=%fused_computation.76 | convolution fusion | flops 4206592 | bytes 550912 | tf_op jit(solution)/shard_map/dot_general | solution.py:55
  15.3 1.9 %fusion.45 = f32[8,512]{1,0:T(8,128)} fusion(bf16[512,512]{1,0:T(8,128)(2,1)} %param.25, f32[512]{0:T(512)} %param.23, bf16[8,512]{1,0:T(8,128)(2,1)} %param.22), kind=kOutput, calls=%fused_computation.75 | convolution fusion | flops 4206592 | bytes 550912 | tf_op jit(solution)/shard_map/dot_general | solution.py:55
  17.1 1.4 fusion.21
  20.3 1.3 dynamic-slice
  22.3 34.1 %all-reduce.8.cloned.1.call-done = (f32[8,512]{1,0:T(8,128)}, f32[8]{0:T(128)}, f32[8,512]{1,0:T(8,128)}, f32[8,512]{1,0:T(8,128)}, f32[8,4]{1,0:T(8,128)}, /*index=5*/f32[8,512]{1,0:T(8,128)}) async-done(((f32[8,512]{1,0:T(8,128)}, f32[8]{0:T(128)}, f32[8,512]{1,0:T(8,128)}, f32[8,512]{1,0:T(8,128)}, f32[8,4]{1,0:T(8,128)}, /*index=5*/f32[8,512]{1,0:T(8,128)}), (f32[8,512]{1,0:T(8,128)}, f32[8]{0:T(128)}, ...) | async-done | bytes 65712
  57.1 0.8 fusion.37
  58.7 1.0 fusion.5
  59.8 0.9 fusion.49
  61.4 0.8 fusion.50
  62.2 1.0 fusion.2
  63.2 0.8 multiply_reduce_fusion.1
  64.0 2.2 %fusion.31 = f32[2,2,1,256]{3,2,1,0:T(1,128)S(1)} fusion(f32[2,2,256,256]{3,2,1,0:T(8,128)} %param.35, f32[2,2,256,1]{2,1,0,3:T(2,128)S(1)} %get-tuple-element.20), kind=kOutput, calls=%fused_computation.46 | convolution fusion | flops 3145728 | bytes 1056768 | tf_op jit(solution)/shard_map/shvd,shd->shv/dot_general | solution.py:105
  66.3 0.8 fusion.39
  67.1 12.0 %all-gather = bf16[4,2,512]{2,1,0:T(2,128)(2,1)S(1)} all-gather(bf16[1,2,512]{2,1,0:T(2,128)(2,1)S(1)} %fusion.39), channel_id=1, replica_groups=mesh['dp'=4,'kv'=4,'tp'=2] {'kv'}, dimensions={0}, use_global_device_ids=true | all-gather | bytes 10240 | tf_op jit(solution)/shard_map/all_gather | solution.py:124
  79.1 0.8 convolution_convert_fusion
  80.0 6.4 %reduce-scatter.3.cloned.1.call-done = bf16[8,256]{1,0:T(8,128)(2,1)} async-done(((bf16[8,512]{1,0:T(8,128)(2,1)}), bf16[8,256]{1,0:T(8,128)(2,1)}) %reduce-scatter.3.cloned.1.call-update) | async-done | bytes 4112 | tf_op jit(solution)/shard_map/reduce_scatter | solution.py:128
  87.0 14.3 %all_gather.7 = bf16[8,2048]{1,0:T(8,128)(2,1)S(1)} all-gather(bf16[8,256]{1,0:T(8,128)(2,1)S(1)} %add_convert_fusion), channel_id=1, replica_groups=mesh['dp'=4,'kv'=4,'tp'=2] {'kv','tp'}, dimensions={1}, use_global_device_ids=true | all-gather | bytes 36864 | tf_op jit(solution)/shard_map/all_gather | solution.py:135
  101.5 2.7 %convolution_multiply_fusion.1 = f32[8,704]{1,0:T(8,128)S(1)} fusion(bf16[2048,704]{0,1:T(8,128)(2,1)} %param.41, bf16[8,2048]{1,0:T(8,128)(2,1)S(1)} %all_gather.7, f32[2048]{0:T(1024)S(1)} %copy-done.3, f32[8]{0:T(128)S(1)} %add_rsqrt_fusion), kind=kOutput, calls=%fused_computation.3 | convolution fusion | flops 23123456 | bytes 2947104 | tf_op jit(solution)/shard_map/dot_general | solution.py:137
  104.2 4.1 %convolution_bitcast_fusion = f32[2048,8]{0,1:T(8,128)} fusion(bf16[704,2048]{1,0:T(8,128)(2,1)S(1)} %copy-done, bf16[2048,704]{0,1:T(8,128)(2,1)} %param.42, bf16[8,2048]{1,0:T(8,128)(2,1)S(1)} %all_gather.7, f32[2048]{0:T(1024)S(1)} %copy-done.3, f32[8,704]{1,0:T(8,128)S(1)} %convolution_multiply_fusion.1, f32[8]{0:T(128)S(1)} %add_rsqrt_fusion), kind=kOutput, calls=%fused_computation | convolution fusion | flops 46225920 | bytes 5896224 | tf_op jit(solution)/shard_map/dot_general | solution.py:144
  108.3 31.5 %reduce-scatter.5.cloned.1.call-done = f32[256,8]{0,1:T(8,128)} async-done(((f32[2048,8]{0,1:T(8,128)}), f32[256,8]{0,1:T(8,128)}) %reduce-scatter.5.cloned.1.call-update) | async-done | bytes 8208 | tf_op jit(solution)/shard_map/reduce_scatter | solution.py:143
  139.8 1.3 fusion.20
  (40 shorter events, 6.7 us)
Async XLA Ops:
  6.5 97.6 %copy-start = (bf16[704,2048]{1,0:T(8,128)(2,1)S(1)}, bf16[704,2048]{1,0:T(8,128)(2,1)}, u32[]{:S(2)}) copy-start(bf16[704,2048]{1,0:T(8,128)(2,1)} %param.43) | copy-start | bytes 8650756
  6.5 73.4 %copy-start.2 = (bf16[8,512]{1,0:T(8,128)(2,1)S(1)}, bf16[8,512]{1,0:T(8,128)(2,1)}, u32[]{:S(2)}) copy-start(bf16[8,512]{1,0:T(8,128)(2,1)} %param.22) | copy-start | bytes 24580
  6.5 72.6 %copy-start.1 = (bf16[512,512]{1,0:T(8,128)(2,1)S(1)}, bf16[512,512]{1,0:T(8,128)(2,1)}, u32[]{:S(2)}) copy-start(bf16[512,512]{1,0:T(8,128)(2,1)} %param.39) | copy-start | bytes 1572868
  6.5 94.9 %copy-start.3 = (f32[2048]{0:T(1024)S(1)}, f32[2048]{0:T(1024)}, u32[]{:S(2)}) copy-start(f32[2048]{0:T(1024)} %param.40) | copy-start | bytes 24580
  6.5 49.8 %all-reduce.8.cloned.1.call-start = ((), (), s32[]{:S(2)}) async-start(), calls=%async_computation.4 | async-start | bytes 140288
  18.6 67.8 %reduce-scatter.3.cloned.1.call-start = ((), (), s32[]{:S(2)}) async-start(), calls=%async_computation.2 | async-start | bytes 12288 | tf_op jit(solution)/shard_map/reduce_scatter | solution.py:128
  19.3 0.7 copy-start.4
  79.9 59.9 %reduce-scatter.5.cloned.1.call-start = ((), (), s32[]{:S(2)}) async-start(), calls=%async_computation.3 | async-start | bytes 73728 | tf_op jit(solution)/shard_map/reduce_scatter | solution.py:143
Sparse Core Ops, SparseCore 0:
  18.7 37.6 all-reduce.7
  80.0 6.2 reduce-scatter.2
  108.4 31.2 reduce-scatter.4
where the time goes:
time: 149 us; the launch traced here: 148 us
  waiting for transfers between devices  71.9 us (48%)
  blocking collectives  26.3 us (18%)
  matrix products  20.6 us (14%)
  between operations  13.8 us (9%)
  other arithmetic  11.7 us (8%)
  local copies, waits for them, and re-layouts  3.11 us (2%)
    unnamed x4, waiting for transfers between devices  34.1 us
    reduce_scatter x1, waiting for transfers between devices, per_device(): lax.psum_scatter(lax.dot_general(down_weight, hidden_units, (((0,), (1,))...  31.5 us
    all_gather x1, blocking collectives, per_device(): lax.all_gather(residual, ('kv', 'tp'), axis=1, tiled=True)  14.3 us
    all_gather x1, blocking collectives, per_device(): lax.all_gather(mixed_heads, 'kv', axis=0, tiled=True)  12 us
    dot_general x5, matrix products, product(): return jnp.dot(normed, weight, preferred_element_type=jnp.float32)  8.84 us
    reduce_scatter x1, waiting for transfers between devices, per_device(): lax.psum_scatter(mix_terms.astype(jnp.bfloat16), 'tp', scatter_dimension=...  6.35 us
    dot_general x1, matrix products, per_device(): lax.dot_general(down_weight, hidden_units, (((0,), (1,)), ((), ())), pref...  4.12 us
  transfers between devices with their start and end apart: 3, of which 3 were waited for; matrix products, arithmetic and copies ran while one was open for 2% of the time, Pallas kernels for 0%

commit v1 on v0

--- a/solution.py
+++ b/solution.py
@@ -1,6 +1,10 @@
+import functools
+
 import jax
 import jax.numpy as jnp
 from jax import lax
+from jax.experimental import pallas as pl
+from jax.experimental.pallas import tpu as pltpu
 from jax.sharding import PartitionSpec as P
 
 EPS = 1e-06
@@ -152,6 +156,456 @@
     return (residual.astype(jnp.float32) + mixer_out).astype(jnp.bfloat16)
 
 
+def cell_kernel(
+    kv_count,
+    tp_count,
+    tokens,
+    pre_gain,
+    query_weight,
+    key_weight,
+    value_weight,
+    outgate_weight,
+    input_gate_weight,
+    forget_gate_weight,
+    cache_keys,
+    cache_values,
+    cache_input,
+    cache_forget,
+    lengths,
+    state_matrix,
+    state_norm,
+    state_max,
+    head_gain,
+    out_weight,
+    mixer_gain,
+    gate_weight,
+    up_weight,
+    down_weight,
+    out,
+    tok_v,
+    pg_v,
+    proj_v,
+    igw_v,
+    fgw_v,
+    ck_v,
+    cv_v,
+    ci_v,
+    cf_v,
+    len_v,
+    sm_v,
+    sn_v,
+    sx_v,
+    hg_v,
+    outw_v,
+    mg_v,
+    gw_v,
+    uw_v,
+    dw_v,
+    hi_v,
+    lo_v,
+    proj_send,
+    proj_recv,
+    tok_recv,
+    mixed_all,
+    half_send,
+    half_recv,
+    down_send,
+    down_recv,
+    local_sem,
+    proj_ssem,
+    proj_rsem,
+    tok_ssem,
+    tok_rsem,
+    mixed_ssem,
+    mixed_rsem,
+    half_ssem,
+    half_rsem,
+    down_ssem,
+    down_rsem,
+):
+    f32, bf16 = jnp.float32, jnp.bfloat16
+    me = lax.axis_index("kv")
+    core = lax.axis_index("tp")
+    rows, width = tok_v.shape
+    own_seqs, block_len = ck_v.shape[0], ck_v.shape[1]
+    head_count, head_size = sn_v.shape[1], sn_v.shape[2]
+    own_width = head_count * head_size
+    model_width = width * kv_count
+    narrow = out.shape[1]
+    peers = [(dk, dt) for dk in range(kv_count) for dt in range(tp_count) if dk or dt]
+    far_first = sorted(range(len(peers)), key=lambda i: -min(peers[i][0], kv_count - peers[i][0]))
+    near_first = far_first[::-1]
+    kv_far = sorted(range(1, kv_count), key=lambda d: -min(d, kv_count - d))
+
+    def peer(dk, dt):
+        return {"kv": lax.rem(me + dk, kv_count), "tp": lax.rem(core + dt, tp_count)}
+
+    sources = (
+        (tokens, tok_v),
+        (pre_gain, pg_v),
+        (query_weight, proj_v.at[0]),
+        (key_weight, proj_v.at[1]),
+        (value_weight, proj_v.at[2]),
+        (outgate_weight, proj_v.at[3]),
+        (input_gate_weight.at[:, pl.ds(pl.multiple_of(me * width, 128), width)], igw_v),
+        (forget_gate_weight.at[:, pl.ds(pl.multiple_of(me * width, 128), width)], fgw_v),
+        (cache_forget, cf_v),
+        (cache_input, ci_v),
+        (lengths, len_v),
+        (state_max, sx_v),
+        (state_norm, sn_v),
+        (head_gain, hg_v),
+        (state_matrix, sm_v),
+        (cache_keys, ck_v),
+        (cache_values, cv_v),
+        (out_weight, outw_v),
+        (mixer_gain, mg_v),
+        (gate_weight, gw_v),
+        (up_weight, uw_v),
+        (down_weight, dw_v),
+    )
+    loads = [
+        pltpu.make_async_copy(src, dst, local_sem.at[i]) for i, (src, dst) in enumerate(sources)
+    ]
+    for load in loads:
+        load.start()
+
+    barrier = pltpu.get_barrier_semaphore()
+    for dk, dt in peers:
+        pl.semaphore_signal(
+            barrier, inc=1, device_id=peer(dk, dt), device_id_type=pl.DeviceIdType.MESH
+        )
+
+    def remote(src, dst, ssem, rsem, dk, dt):
+        return pltpu.make_async_remote_copy(
+            src_ref=src,
+            dst_ref=dst,
+            send_sem=ssem,
+            recv_sem=rsem,
+            device_id=peer(dk, dt),
+            device_id_type=pl.DeviceIdType.MESH,
+        )
+
+    for i in range(2):
+        loads[i].wait()
+    token_values = tok_v[...].astype(f32)
+    squares = jnp.sum(token_values * token_values, axis=1, keepdims=True)
+    normed = (token_values * pg_v[...]).astype(bf16)
+    for i in range(4):
+        loads[2 + i].wait()
+        term = jnp.dot(normed, proj_v[i], preferred_element_type=f32)
+        for r in range(kv_count):
+            proj_send[r, own_seqs * i : own_seqs * (i + 1), :own_width] = term[
+                own_seqs * r : own_seqs * (r + 1), :
+            ]
+    loads[6].wait()
+    loads[7].wait()
+    contract_last = (((1,), (1,)), ((), ()))
+    gates = [
+        lax.dot_general(normed, ref[...], contract_last, preferred_element_type=f32)
+        for ref in (igw_v, fgw_v)
+    ]
+    lane = lax.broadcasted_iota(jnp.int32, (rows, 128), 1)
+    small = jnp.where(lane == 2 * head_count, squares, 0.0)
+    for g in range(2):
+        for h in range(head_count):
+            column = gates[g][:, h : h + 1]
+            for t in range(1, tp_count):
+                at = t * head_count + h
+                column = jnp.where(core == t, gates[g][:, at : at + 1], column)
+            small = jnp.where(lane == g * head_count + h, column, small)
+    for r in range(kv_count):
+        for i in range(4):
+            proj_send[r, own_seqs * i : own_seqs * (i + 1), own_width:] = small[
+                own_seqs * r : own_seqs * (r + 1), :
+            ]
+
+    pl.semaphore_wait(barrier, len(peers))
+    proj_copies = {}
+    for d in kv_far:
+        proj_copies[d] = remote(
+            proj_send.at[lax.rem(me + d, kv_count)],
+            proj_recv.at[d - 1],
+            proj_ssem.at[d - 1],
+            proj_rsem.at[d - 1],
+            d,
+            0,
+        )
+        proj_copies[d].start()
+    tok_copies = {}
+    for d in kv_far:
+        tok_copies[d] = remote(
+            tok_v, tok_recv.at[d - 1], tok_ssem.at[d - 1], tok_rsem.at[d - 1], d, 0
+        )
+        tok_copies[d].start()
+
+    for i in range(8, 15):
+        loads[i].wait()
+    for s in range(own_seqs):
+        for h in range(head_count):
+            whole = sm_v[s, h]
+            high = whole.astype(bf16)
+            hi_v[s, h] = high
+            lo_v[s, h] = (whole - high.astype(f32)).astype(bf16)
+    at_row = lax.broadcasted_iota(jnp.int32, (block_len, block_len), 0)
+    at_col = lax.broadcasted_iota(jnp.int32, (block_len, block_len), 1)
+    position_row = lax.broadcasted_iota(jnp.int32, (1, block_len), 1)
+    base_log, base_max, base_total = {}, {}, {}
+    for s in range(own_seqs):
+        length = len_v[0:1, s : s + 1]
+        forget_all = cf_v[s]
+        input_all = ci_v[s]
+        for h in range(head_count):
+            forget_column = jnp.broadcast_to(forget_all[:, h : h + 1], (block_len, block_len))
+            input_column = jnp.broadcast_to(input_all[:, h : h + 1], (block_len, block_len))
+            counted = (at_row <= at_col) & (at_row < length)
+            running = jnp.sum(jnp.where(counted, forget_column, 0.0), axis=0, keepdims=True)
+            inputs = jnp.sum(
+                jnp.where(at_row == at_col, input_column, 0.0), axis=0, keepdims=True
+            )
+            total = running[:, block_len - 1 : block_len]
+            logs = jnp.where(position_row < length, total - running + inputs, -jnp.inf)
+            base_log[s, h] = logs
+            base_max[s, h] = jnp.max(logs, axis=1, keepdims=True)
+            base_total[s, h] = total
+    for i in range(15, 17):
+        loads[i].wait()
+
+    summed = proj_send[me]
+    for d in range(1, kv_count):
+        proj_copies[d].wait_recv()
+        summed = summed + proj_recv[d - 1]
+    inv_root = head_size ** (-0.5)
+    mixed_rows = []
+    for s in range(own_seqs):
+        tail = summed[s : s + 1, own_width:]
+        square = tail[:, 2 * head_count : 2 * head_count + 1]
+        scale_first = lax.rsqrt(square / model_width + EPS)
+        tail = tail * scale_first
+        query, key, value, outgate = (
+            (scale_first * summed[own_seqs * i + s : own_seqs * i + s + 1, :own_width])
+            .astype(bf16)
+            .astype(f32)
+            for i in range(4)
+        )
+        query = query * inv_root
+        hidden_parts = []
+        for h in range(head_count):
+            cols = slice(h * head_size, (h + 1) * head_size)
+            in_gate = tail[:, h : h + 1]
+            forget_arg = tail[:, head_count + h : head_count + h + 1]
+            forget_new = jnp.minimum(forget_arg, 0.0) - jnp.log1p(jnp.exp(-jnp.abs(forget_arg)))
+            state_log = base_total[s, h] + forget_new + sx_v[s : s + 1, h : h + 1]
+            peak_log = jnp.maximum(
+                jnp.maximum(state_log, in_gate), base_max[s, h] + forget_new
+            )
+            q = query[:, cols]
+            q_low = q.astype(bf16)
+            dots = lax.dot_general(
+                q_low, ck_v[s, :, cols], contract_last, preferred_element_type=f32
+            )
+            scores = jnp.exp(base_log[s, h] + forget_new - peak_log) * dots
+            self_score = jnp.exp(in_gate - peak_log) * jnp.sum(
+                q * key[:, cols], axis=1, keepdims=True
+            )
+            carried = jnp.exp(state_log - peak_log)
+            read = lax.dot_general(
+                q_low, hi_v[s, h], contract_last, preferred_element_type=f32
+            ) + lax.dot_general(q_low, lo_v[s, h], contract_last, preferred_element_type=f32)
+            norm_read = jnp.sum(sn_v[s, h : h + 1, :] * q, axis=1, keepdims=True)
+            numerator = (
+                carried * read
+                + jnp.dot(scores.astype(bf16), cv_v[s, :, cols], preferred_element_type=f32)
+                + self_score * value[:, cols]
+            )
+            denominator = (
+                carried * norm_read + jnp.sum(scores, axis=1, keepdims=True) + self_score
+            )
+            hidden = numerator / jnp.maximum(jnp.abs(denominator), 1.0)
+            hidden_parts.append(hidden * hg_v[:, cols] * jax.nn.sigmoid(outgate[:, cols]))
+        mixed_rows.append(jnp.concatenate(hidden_parts, axis=1))
+    for s in range(own_seqs):
+        mixed_all[me, s : s + 1, :] = mixed_rows[s].astype(bf16).astype(f32)
+    mixed_copies = {}
+    for d in kv_far:
+        mixed_copies[d] = remote(
+            mixed_all.at[me],
+            mixed_all.at[me],
+            mixed_ssem.at[d - 1],
+            mixed_rsem.at[lax.rem(me + 0, kv_count)],
+            d,
+            0,
+        )
+        mixed_copies[d].start()
+    loads[17].wait()
+    for d in range(1, kv_count):
+        source = lax.rem(me + kv_count - d, kv_count)
+        remote(
+            mixed_all.at[source], mixed_all.at[source], mixed_ssem.at[d - 1],
+            mixed_rsem.at[source], d, 0,
+        ).wait_recv()
+    mixed = jnp.concatenate([mixed_all[r] for r in range(kv_count)], axis=0).astype(bf16)
+    own_half = jnp.dot(mixed, outw_v[...], preferred_element_type=f32).astype(bf16)
+    half_send[...] = own_half
+    half_copies = {}
+    for i in far_first:
+        dk, dt = peers[i]
+        half_copies[i] = remote(
+            half_send, half_recv.at[i], half_ssem.at[i], half_rsem.at[i], dk, dt
+        )
+        half_copies[i].start()
+    for i in range(18, 21):
+        loads[i].wait()
+    sum_squares = jnp.zeros((rows, 1), f32)
+    gate_acc = jnp.zeros((rows, gw_v.shape[1]), f32)
+    up_acc = jnp.zeros((rows, gw_v.shape[1]), f32)
+    own_residual = None
+    for dk in sorted(range(kv_count), key=lambda d: min(d, kv_count - d)):
+        source = lax.rem(me + kv_count - dk, kv_count)
+        halves = [own_half.astype(f32)] if dk == 0 else []
+        for i, (pk, pt) in enumerate(peers):
+            if pk == dk:
+                half_copies[i].wait_recv()
+                halves.append(half_recv[i].astype(f32))
+        if dk:
+            tok_copies[dk].wait_recv()
+            chunk_tokens = tok_recv[dk - 1].astype(f32)
+        else:
+            chunk_tokens = token_values
+        residual = (chunk_tokens + sum(halves[1:], halves[0])).astype(bf16).astype(f32)
+        if dk == 0:
+            own_residual = residual
+        sum_squares = sum_squares + jnp.sum(residual * residual, axis=1, keepdims=True)
+        at = pl.multiple_of(source * width, 128)
+        normed_mid = (residual * mg_v[:, pl.ds(at, width)]).astype(bf16)
+        gate_acc = gate_acc + jnp.dot(
+            normed_mid, gw_v[pl.ds(at, width), :], preferred_element_type=f32
+        )
+        up_acc = up_acc + jnp.dot(
+            normed_mid, uw_v[pl.ds(at, width), :], preferred_element_type=f32
+        )
+    scale_mid = lax.rsqrt(sum_squares / model_width + EPS)
+    hidden_units = (jax.nn.silu(scale_mid * gate_acc) * (scale_mid * up_acc)).astype(bf16)
+    loads[21].wait()
+
+    def down_part(dk, dt):
+        target = lax.rem(me + dk, kv_count) * tp_count + lax.rem(core + dt, tp_count)
+        at = pl.multiple_of(target * narrow, 128)
+        return jnp.dot(hidden_units, dw_v[:, pl.ds(at, narrow)], preferred_element_type=f32)
+
+    down_copies = {}
+    for i in far_first:
+        dk, dt = peers[i]
+        down_send[i] = down_part(dk, dt).astype(down_send.dtype)
+        down_copies[i] = remote(
+            down_send.at[i], down_recv.at[i], down_ssem.at[i], down_rsem.at[i], dk, dt
+        )
+        down_copies[i].start()
+    total_out = own_residual[:, :narrow]
+    for t in range(1, tp_count):
+        total_out = jnp.where(
+            core == t, own_residual[:, t * narrow : (t + 1) * narrow], total_out
+        )
+    mixer_out = down_part(0, 0)
+    for i in near_first:
+        down_copies[i].wait_recv()
+        mixer_out = mixer_out + down_recv[i].astype(f32)
+    out[...] = (total_out + mixer_out).astype(out.dtype)
+
+    for copies in (proj_copies, tok_copies, mixed_copies, half_copies, down_copies):
+        for copy in copies.values():
+            copy.wait_send()
+
+
+def fused_device(mesh, *args):
+    (tokens, pre_gain, query_weight, _, _, _, input_gate_weight, forget_gate_weight) = args[:8]
+    cache_keys, cache_values, cache_input, cache_forget, lengths = args[8:13]
+    state_matrix, state_norm, state_max, head_gain, out_weight = args[13:18]
+    mixer_gain, gate_weight, up_weight, down_weight = args[18:]
+    kv_count, tp_count = mesh.shape["kv"], mesh.shape["tp"]
+    f32, bf16 = jnp.float32, jnp.bfloat16
+    rows, width = tokens.shape
+    own_seqs = cache_keys.shape[0]
+    own_width = query_weight.shape[1]
+    narrow = width // tp_count
+    peer_count = kv_count * tp_count - 1
+    given = list(args)
+    given[1] = pre_gain[None, :]
+    given[6] = input_gate_weight.T
+    given[7] = forget_gate_weight.T
+    given[12] = lengths[None, :]
+    given[16] = head_gain[None, :]
+    given[18] = mixer_gain[None, :]
+
+    def held(array):
+        return pltpu.VMEM(array.shape, array.dtype)
+
+    gate_heads = input_gate_weight.shape[1]
+    dma = pltpu.SemaphoreType.DMA
+    scratch = [
+        held(tokens),
+        held(given[1]),
+        pltpu.VMEM((4,) + query_weight.shape, bf16),
+        pltpu.VMEM((gate_heads, width), bf16),
+        pltpu.VMEM((gate_heads, width), bf16),
+        held(cache_keys),
+        held(cache_values),
+        held(cache_input),
+        held(cache_forget),
+        held(given[12]),
+        held(state_matrix),
+        held(state_norm),
+        held(state_max),
+        held(given[16]),
+        held(out_weight),
+        held(given[18]),
+        held(gate_weight),
+        held(up_weight),
+        held(down_weight),
+        pltpu.VMEM(state_matrix.shape, bf16),
+        pltpu.VMEM(state_matrix.shape, bf16),
+        pltpu.VMEM((kv_count, 4 * own_seqs, own_width + 128), f32),
+        pltpu.VMEM((kv_count - 1, 4 * own_seqs, own_width + 128), f32),
+        pltpu.VMEM((kv_count - 1, rows, width), bf16),
+        pltpu.VMEM((kv_count, own_seqs, own_width), f32),
+        pltpu.VMEM((rows, width), bf16),
+        pltpu.VMEM((peer_count, rows, width), bf16),
+        pltpu.VMEM((peer_count, rows, narrow), f32),
+        pltpu.VMEM((peer_count, rows, narrow), f32),
+        dma((len(args),)),
+        dma((kv_count - 1,)),
+        dma((kv_count - 1,)),
+        dma((kv_count - 1,)),
+        dma((kv_count - 1,)),
+        dma((kv_count - 1,)),
+        dma((kv_count,)),
+        dma((peer_count,)),
+        dma((peer_count,)),
+        dma((peer_count,)),
+        dma((peer_count,)),
+    ]
+    return pl.pallas_call(
+        functools.partial(cell_kernel, kv_count, tp_count),
+        out_shape=jax.ShapeDtypeStruct((rows, narrow), tokens.dtype),
+        in_specs=[pl.BlockSpec(memory_space=pl.ANY)] * len(args),
+        out_specs=pl.BlockSpec(memory_space=pltpu.VMEM),
+        scratch_shapes=scratch,
+        compiler_params=pltpu.CompilerParams(
+            collective_id=0, has_side_effects=True, vmem_limit_bytes=60 * 1024 * 1024
+        ),
+    )(*given)
+
+
+def fits_tiles(mesh, tokens, query_weight, cache_keys, state_norm):
+    kv_count, tp_count = mesh.shape["kv"], mesh.shape["tp"]
+    return (
+        tokens.shape[1] % (kv_count * tp_count * 128) == 0
+        and query_weight.shape[1] % (tp_count * 128) == 0
+        and state_norm.shape[2] % 128 == 0
+        and kv_count > 1
+    )
+
+
 def solution(mesh):
     in_specs = (
         P("dp", "kv"),
@@ -178,6 +632,12 @@
         P(("kv", "tp"), None),
     )
     out_specs = P("dp", ("kv", "tp"))
-    return jax.shard_map(
-        per_device, mesh=mesh, in_specs=in_specs, out_specs=out_specs, check_vma=False
-    )
+
+    def run(*args):
+        fused = fits_tiles(mesh, args[0], args[2], args[8], args[14])
+        body = functools.partial(fused_device, mesh) if fused else per_device
+        return jax.shard_map(
+            body, mesh=mesh, in_specs=in_specs, out_specs=out_specs, check_vma=False
+        )(*args)
+
+    return run

time: 149 us -> 36 us (0.24)
  waiting for transfers between devices: 71.9 us -> 0 us
  blocking collectives: 26.3 us -> 0 us
  Pallas kernels: 0 us -> 24 us
  matrix products: 20.6 us -> 0 us
  between operations: 13.8 us -> 0.01 us
  other arithmetic: 11.7 us -> 0 us
  local copies, waits for them, and re-layouts: 3.11 us -> 11.7 us
    reduce_scatter x2 -> x0, waiting for transfers between devices: 37.8 us -> none  [the longest x1 31.5 us: per_device(): lax.psum_scatter(lax.dot_general(down_weight, hidden_units, (((0,), (1,))...]
    unnamed x4 -> x0, waiting for transfers between devices: 34.1 us -> none
    all_gather x2 -> x0, blocking collectives: 26.3 us -> none  [the longest x1 14.3 us: per_device(): lax.all_gather(residual, ('kv', 'tp'), axis=1, tiled=True)]
    pallas_call x0 -> x1, Pallas kernels: none -> 24 us  [fused_device(): pl.pallas_call(functools.partial(cell_kernel, kv_count, tp_count), out_sh...]
    dot_general x11 -> x0, matrix products: 20.6 us -> none  [the longest x5 8.84 us: product(): return jnp.dot(normed, weight, preferred_element_type=jnp.float32)]
    unnamed x13 -> x7, local copies, waits for them, and re-layouts: 1.35 us -> 11.7 us
    convert_element_type x4 -> x0, other arithmetic: 2.8 us -> none  [the longest x1 1.29 us: per_device(): return (residual.astype(jnp.float32) + mixer_out).astype(jnp.bfloat16)]
    reduce_sum x3 -> x0, other arithmetic: 2.55 us -> none  [the longest x1 1.57 us: per_device(): squares = jnp.sum(token_values * token_values, axis=1)]
  transfers between devices with their start and end apart: 3 -> 0, of which waited for: 3 -> 0; matrix products, arithmetic and copies ran while one was open for 2% -> 0% of each run, Pallas kernels for 0% -> 0%
where the time goes in v1:
time: 36 us; the launch traced here: 35.7 us
  Pallas kernels  24 us (67%)
  local copies, waits for them, and re-layouts  11.7 us (32%)
    pallas_call x1, Pallas kernels, fused_device(): pl.pallas_call(functools.partial(cell_kernel, kv_count, tp_count), out_sh...  24 us
    unnamed x7, local copies, waits for them, and re-layouts  11.7 us

profile of v1, /device:TPU:0, one launch (start us, length us, event | category | flops | bytes accessed | tf_op | source)
XLA Modules:
  0.0 35.7 jit_solution(9414099283598167900)
XLA Ops:
  0.0 1.4 %copy.23.cache_input = f32[2,64,2]{2,1,0:T(8,128)} copy(f32[2,64,2]{1,2,0:T(2,128)} %param.32) | data formatting | bytes 2048 | tf_op args[10]
  1.4 1.4 %copy.24.cache_forget = f32[2,64,2]{2,1,0:T(8,128)} copy(f32[2,64,2]{1,2,0:T(2,128)} %param.33) | data formatting | bytes 2048 | tf_op args[11]
  2.8 0.0 copy-start
  2.8 4.7 %copy.25.gate_weight = bf16[2048,704]{1,0:T(8,128)(2,1)} copy(bf16[2048,704]{0,1:T(8,128)(2,1)} %param.41) | data formatting | bytes 5767168 | tf_op args[19]
  7.6 0.0 copy-done
  7.6 2.8 %copy.26.up_weight = bf16[2048,704]{1,0:T(8,128)(2,1)} copy(bf16[2048,704]{0,1:T(8,128)(2,1)S(1)} %copy-done) | data formatting | bytes 5767168 | tf_op args[20]
  10.4 24.0 %shard_map.208 = bf16[8,256]{1,0:T(8,128)(2,1)} custom-call(bf16[8,512]{1,0:T(8,128)(2,1)} %tokens.1, f32[1,512]{1,0:T(1,128)} %bitcast.9, bf16[512,512]{1,0:T(8,128)(2,1)} %query_weight.1, bf16[512,512]{1,0:T(8,128)(2,1)} %key_weight.1, bf16[512,512]{1,0:T(8,128)(2,1)} %value_weight.1, bf16[512,512]{1,0:T(8,128)(2,1)} %outgate_weight.1, ...), custom_call_target="tpu_custom_call" | custom-call | tf_op jit(solution)/shard_map/pallas_call | solution.py:587
  34.4 1.3 %copy.28 = bf16[8,256]{1,0:T(8,128)(2,1)} copy(bf16[8,256]{1,0:T(8,128)(2,1)} %shard_map.208) | data formatting | bytes 8192
Async XLA Ops:
  2.8 4.8 %copy-start = (bf16[2048,704]{0,1:T(8,128)(2,1)S(1)}, bf16[2048,704]{0,1:T(8,128)(2,1)}, u32[]{:S(2)}) copy-start(bf16[2048,704]{0,1:T(8,128)(2,1)} %param.42) | copy-start | bytes 8650756

commit v2 on v1

--- a/solution.py
+++ b/solution.py
@@ -267,7 +267,7 @@
     loads = [
         pltpu.make_async_copy(src, dst, local_sem.at[i]) for i, (src, dst) in enumerate(sources)
     ]
-    for load in loads:
+    for load in loads[:8]:
         load.start()
 
     barrier = pltpu.get_barrier_semaphore()
@@ -300,6 +300,8 @@
             ]
     loads[6].wait()
     loads[7].wait()
+    for load in loads[8:]:
+        load.start()
     contract_last = (((1,), (1,)), ((), ()))
     gates = [
         lax.dot_general(normed, ref[...], contract_last, preferred_element_type=f32)
@@ -350,21 +352,20 @@
     at_row = lax.broadcasted_iota(jnp.int32, (block_len, block_len), 0)
     at_col = lax.broadcasted_iota(jnp.int32, (block_len, block_len), 1)
     position_row = lax.broadcasted_iota(jnp.int32, (1, block_len), 1)
+    up_to = (at_row <= at_col).astype(f32)
     base_log, base_max, base_total = {}, {}, {}
     for s in range(own_seqs):
-        length = len_v[0:1, s : s + 1]
-        forget_all = cf_v[s]
-        input_all = ci_v[s]
+        live = position_row < len_v[0:1, s : s + 1]
+        running_all = jnp.dot(
+            jnp.where(live, cf_v[s], 0.0),
+            up_to,
+            precision=lax.Precision.HIGHEST,
+            preferred_element_type=f32,
+        )
         for h in range(head_count):
-            forget_column = jnp.broadcast_to(forget_all[:, h : h + 1], (block_len, block_len))
-            input_column = jnp.broadcast_to(input_all[:, h : h + 1], (block_len, block_len))
-            counted = (at_row <= at_col) & (at_row < length)
-            running = jnp.sum(jnp.where(counted, forget_column, 0.0), axis=0, keepdims=True)
-            inputs = jnp.sum(
-                jnp.where(at_row == at_col, input_column, 0.0), axis=0, keepdims=True
-            )
+            running = running_all[h : h + 1, :]
             total = running[:, block_len - 1 : block_len]
-            logs = jnp.where(position_row < length, total - running + inputs, -jnp.inf)
+            logs = jnp.where(live, total - running + ci_v[s, h : h + 1, :], -jnp.inf)
             base_log[s, h] = logs
             base_max[s, h] = jnp.max(logs, axis=1, keepdims=True)
             base_total[s, h] = total
@@ -457,8 +458,8 @@
     for i in range(18, 21):
         loads[i].wait()
     sum_squares = jnp.zeros((rows, 1), f32)
-    gate_acc = jnp.zeros((rows, gw_v.shape[1]), f32)
-    up_acc = jnp.zeros((rows, gw_v.shape[1]), f32)
+    gate_acc = jnp.zeros((rows, gw_v.shape[0]), f32)
+    up_acc = jnp.zeros((rows, gw_v.shape[0]), f32)
     own_residual = None
     for dk in sorted(range(kv_count), key=lambda d: min(d, kv_count - d)):
         source = lax.rem(me + kv_count - dk, kv_count)
@@ -478,11 +479,11 @@
         sum_squares = sum_squares + jnp.sum(residual * residual, axis=1, keepdims=True)
         at = pl.multiple_of(source * width, 128)
         normed_mid = (residual * mg_v[:, pl.ds(at, width)]).astype(bf16)
-        gate_acc = gate_acc + jnp.dot(
-            normed_mid, gw_v[pl.ds(at, width), :], preferred_element_type=f32
-        )
-        up_acc = up_acc + jnp.dot(
-            normed_mid, uw_v[pl.ds(at, width), :], preferred_element_type=f32
+        gate_acc = gate_acc + lax.dot_general(
+            normed_mid, gw_v[:, pl.ds(at, width)], contract_last, preferred_element_type=f32
+        )
+        up_acc = up_acc + lax.dot_general(
+            normed_mid, uw_v[:, pl.ds(at, width)], contract_last, preferred_element_type=f32
         )
     scale_mid = lax.rsqrt(sum_squares / model_width + EPS)
     hidden_units = (jax.nn.silu(scale_mid * gate_acc) * (scale_mid * up_acc)).astype(bf16)
@@ -534,8 +535,12 @@
     given[6] = input_gate_weight.T
     given[7] = forget_gate_weight.T
     given[12] = lengths[None, :]
+    given[10] = jnp.swapaxes(cache_input, 1, 2)
+    given[11] = jnp.swapaxes(cache_forget, 1, 2)
     given[16] = head_gain[None, :]
     given[18] = mixer_gain[None, :]
+    given[19] = gate_weight.T
+    given[20] = up_weight.T
 
     def held(array):
         return pltpu.VMEM(array.shape, array.dtype)
@@ -550,8 +555,8 @@
         pltpu.VMEM((gate_heads, width), bf16),
         held(cache_keys),
         held(cache_values),
-        held(cache_input),
-        held(cache_forget),
+        held(given[10]),
+        held(given[11]),
         held(given[12]),
         held(state_matrix),
         held(state_norm),
@@ -559,8 +564,8 @@
         held(given[16]),
         held(out_weight),
         held(given[18]),
-        held(gate_weight),
-        held(up_weight),
+        held(given[19]),
+        held(given[20]),
         held(down_weight),
         pltpu.VMEM(state_matrix.shape, bf16),
         pltpu.VMEM(state_matrix.shape, bf16),
@@ -570,8 +575,8 @@
         pltpu.VMEM((kv_count, own_seqs, own_width), f32),
         pltpu.VMEM((rows, width), bf16),
         pltpu.VMEM((peer_count, rows, width), bf16),
-        pltpu.VMEM((peer_count, rows, narrow), f32),
-        pltpu.VMEM((peer_count, rows, narrow), f32),
+        pltpu.VMEM((peer_count, rows, narrow), bf16),
+        pltpu.VMEM((peer_count, rows, narrow), bf16),
         dma((len(args),)),
         dma((kv_count - 1,)),
         dma((kv_count - 1,)),

time: 36 us -> 25.9 us (0.72)
  local copies, waits for them, and re-layouts: 11.7 us -> 1.28 us
  Pallas kernels: 24 us -> 24.4 us
    unnamed x7 -> x1, local copies, waits for them, and re-layouts: 11.7 us -> 1.28 us
    pallas_call x1, Pallas kernels: 24 us -> 24.4 us  [fused_device(): pl.pallas_call(functools.partial(cell_kernel, kv_count, tp_count), out_sh...]
where the time goes in v2:
time: 25.9 us; the launch traced here: 25.7 us
  Pallas kernels  24.4 us (94%)
  local copies, waits for them, and re-layouts  1.28 us (5%)
    pallas_call x1, Pallas kernels, fused_device(): pl.pallas_call(functools.partial(cell_kernel, kv_count, tp_count), out_sh...  24.4 us
    unnamed x1, local copies, waits for them, and re-layouts  1.28 us

profile of v2, /device:TPU:0, one launch (start us, length us, event | category | flops | bytes accessed | tf_op | source)
XLA Modules:
  0.0 25.7 jit_solution(6680789881998908973)
XLA Ops:
  0.0 24.4 %shard_map.208 = bf16[8,256]{1,0:T(8,128)(2,1)} custom-call(bf16[8,512]{1,0:T(8,128)(2,1)} %tokens.1, f32[1,512]{1,0:T(1,128)} %bitcast.15, bf16[512,512]{1,0:T(8,128)(2,1)} %query_weight.1, bf16[512,512]{1,0:T(8,128)(2,1)} %key_weight.1, bf16[512,512]{1,0:T(8,128)(2,1)} %value_weight.1, bf16[512,512]{1,0:T(8,128)(2,1)} %outgate_weight.1, ...), custom_call_target="tpu_custom_call" | custom-call | tf_op jit(solution)/shard_map/pallas_call | solution.py:592
  24.4 1.3 %copy.24 = bf16[8,256]{1,0:T(8,128)(2,1)} copy(bf16[8,256]{1,0:T(8,128)(2,1)} %shard_map.208) | data formatting | bytes 8192

commit v3 on v2

--- a/solution.py
+++ b/solution.py
@@ -205,6 +205,9 @@
     lo_v,
     proj_send,
     proj_recv,
+    proj_own,
+    small_send,
+    small_recv,
     tok_recv,
     mixed_all,
     half_send,
@@ -214,6 +217,8 @@
     local_sem,
     proj_ssem,
     proj_rsem,
+    small_ssem,
+    small_rsem,
     tok_ssem,
     tok_rsem,
     mixed_ssem,
@@ -291,13 +296,16 @@
     token_values = tok_v[...].astype(f32)
     squares = jnp.sum(token_values * token_values, axis=1, keepdims=True)
     normed = (token_values * pg_v[...]).astype(bf16)
+    terms = []
     for i in range(4):
         loads[2 + i].wait()
-        term = jnp.dot(normed, proj_v[i], preferred_element_type=f32)
-        for r in range(kv_count):
-            proj_send[r, own_seqs * i : own_seqs * (i + 1), :own_width] = term[
-                own_seqs * r : own_seqs * (r + 1), :
-            ]
+        terms.append(jnp.dot(normed, proj_v[i], preferred_element_type=f32))
+    for r in range(kv_count):
+        block = jnp.concatenate(
+            [term[own_seqs * r : own_seqs * (r + 1), :] for term in terms], axis=0
+        )
+        proj_send[r] = block.astype(proj_send.dtype)
+        proj_own[r] = block
     loads[6].wait()
     loads[7].wait()
     for load in loads[8:]:
@@ -317,10 +325,7 @@
                 column = jnp.where(core == t, gates[g][:, at : at + 1], column)
             small = jnp.where(lane == g * head_count + h, column, small)
     for r in range(kv_count):
-        for i in range(4):
-            proj_send[r, own_seqs * i : own_seqs * (i + 1), own_width:] = small[
-                own_seqs * r : own_seqs * (r + 1), :
-            ]
+        small_send[r] = jnp.concatenate([small[own_seqs * r : own_seqs * (r + 1), :]] * 4, axis=0)
 
     pl.semaphore_wait(barrier, len(peers))
     proj_copies = {}
@@ -334,6 +339,17 @@
             0,
         )
         proj_copies[d].start()
+    small_copies = {}
+    for d in kv_far:
+        small_copies[d] = remote(
+            small_send.at[lax.rem(me + d, kv_count)],
+            small_recv.at[d - 1],
+            small_ssem.at[d - 1],
+            small_rsem.at[d - 1],
+            d,
+            0,
+        )
+        small_copies[d].start()
     tok_copies = {}
     for d in kv_far:
         tok_copies[d] = remote(
@@ -372,19 +388,22 @@
     for i in range(15, 17):
         loads[i].wait()
 
-    summed = proj_send[me]
+    summed = proj_own[me]
+    tails = small_send[me]
     for d in range(1, kv_count):
         proj_copies[d].wait_recv()
-        summed = summed + proj_recv[d - 1]
+        summed = summed + proj_recv[d - 1].astype(f32)
+        small_copies[d].wait_recv()
+        tails = tails + small_recv[d - 1]
     inv_root = head_size ** (-0.5)
     mixed_rows = []
     for s in range(own_seqs):
-        tail = summed[s : s + 1, own_width:]
+        tail = tails[s : s + 1, :]
         square = tail[:, 2 * head_count : 2 * head_count + 1]
         scale_first = lax.rsqrt(square / model_width + EPS)
         tail = tail * scale_first
         query, key, value, outgate = (
-            (scale_first * summed[own_seqs * i + s : own_seqs * i + s + 1, :own_width])
+            (scale_first * summed[own_seqs * i + s : own_seqs * i + s + 1, :])
             .astype(bf16)
             .astype(f32)
             for i in range(4)
@@ -513,7 +532,7 @@
         mixer_out = mixer_out + down_recv[i].astype(f32)
     out[...] = (total_out + mixer_out).astype(out.dtype)
 
-    for copies in (proj_copies, tok_copies, mixed_copies, half_copies, down_copies):
+    for copies in (proj_copies, small_copies, tok_copies, mixed_copies, half_copies, down_copies):
         for copy in copies.values():
             copy.wait_send()
 
@@ -569,8 +588,11 @@
         held(down_weight),
         pltpu.VMEM(state_matrix.shape, bf16),
         pltpu.VMEM(state_matrix.shape, bf16),
-        pltpu.VMEM((kv_count, 4 * own_seqs, own_width + 128), f32),
-        pltpu.VMEM((kv_count - 1, 4 * own_seqs, own_width + 128), f32),
+        pltpu.VMEM((kv_count, 4 * own_seqs, own_width), bf16),
+        pltpu.VMEM((kv_count - 1, 4 * own_seqs, own_width), bf16),
+        pltpu.VMEM((kv_count, 4 * own_seqs, own_width), f32),
+        pltpu.VMEM((kv_count, 4 * own_seqs, 128), f32),
+        pltpu.VMEM((kv_count - 1, 4 * own_seqs, 128), f32),
         pltpu.VMEM((kv_count - 1, rows, width), bf16),
         pltpu.VMEM((kv_count, own_seqs, own_width), f32),
         pltpu.VMEM((rows, width), bf16),
@@ -578,6 +600,8 @@
         pltpu.VMEM((peer_count, rows, narrow), bf16),
         pltpu.VMEM((peer_count, rows, narrow), bf16),
         dma((len(args),)),
+        dma((kv_count - 1,)),
+        dma((kv_count - 1,)),
         dma((kv_count - 1,)),
         dma((kv_count - 1,)),
         dma((kv_count - 1,)),

time: 25.9 us -> 25.4 us (0.981)
  Pallas kernels: 24.4 us -> 23.9 us
    pallas_call x1, Pallas kernels: 24.4 us -> 23.9 us  [fused_device(): pl.pallas_call(functools.partial(cell_kernel, kv_count, tp_count), out_sh...]
where the time goes in v3:
time: 25.4 us; the launch traced here: 25.2 us
  Pallas kernels  23.9 us (94%)
  local copies, waits for them, and re-layouts  1.28 us (5%)
    pallas_call x1, Pallas kernels, fused_device(): pl.pallas_call(functools.partial(cell_kernel, kv_count, tp_count), out_sh...  23.9 us
    unnamed x1, local copies, waits for them, and re-layouts  1.28 us

profile of v3, /device:TPU:0, one launch (start us, length us, event | category | flops | bytes accessed | tf_op | source)
XLA Modules:
  0.0 25.2 jit_solution(13086363313454486647)
XLA Ops:
  0.0 23.9 %shard_map.208 = bf16[8,256]{1,0:T(8,128)(2,1)} custom-call(bf16[8,512]{1,0:T(8,128)(2,1)} %tokens.1, f32[1,512]{1,0:T(1,128)} %bitcast.15, bf16[512,512]{1,0:T(8,128)(2,1)} %query_weight.1, bf16[512,512]{1,0:T(8,128)(2,1)} %key_weight.1, bf16[512,512]{1,0:T(8,128)(2,1)} %value_weight.1, bf16[512,512]{1,0:T(8,128)(2,1)} %outgate_weight.1, ...), custom_call_target="tpu_custom_call" | custom-call | tf_op jit(solution)/shard_map/pallas_call | solution.py:616
  23.9 1.3 %copy.24 = bf16[8,256]{1,0:T(8,128)(2,1)} copy(bf16[8,256]{1,0:T(8,128)(2,1)} %shard_map.208) | data formatting | bytes 8192
